TPU v7x, 32 devices: a whole 2x2x4 slice. The times are simulated.
32 devices in a mesh: sp: 8 (over z, x), dp: 4 (over y, core).
Axes of the slice: x: 2, y: 2, z: 4, core: 2. Of those that a mesh axis runs over, the one named last changes fastest.
Arguments:
- normed_input: bfloat16 [2560, 2048], P('sp'), may hold values from -6 to 6
- out_grad: bfloat16 [2560, 2048], P('sp'), may hold values from -6 to 6
- value_weight: bfloat16 [2048, 1024], P(None, 'dp'), may hold values from -0.125 to 0.125
- gate_weight: bfloat16 [2048, 1024], P(None, 'dp'), may hold values from -0.125 to 0.125
- down_weight: bfloat16 [1024, 2048], P('dp'), may hold values from -0.1875 to 0.1875
- conv_kernel: float32 [31, 1024], P(None, 'dp'), may hold values from -5 to 5
- conv_bias: float32 [1024], P('dp'), may hold values from -3 to 3
- norm_gain: float32 [1024], P('dp'), may hold values from 0.1 to 1.9
- norm_shift: float32 [1024], P('dp'), may hold values from -3 to 3
Outputs:
- input_grad: bfloat16 [2560, 2048], P('sp')
- value_grad: float32 [2048, 1024], P('sp', 'dp')
- gate_grad: float32 [2048, 1024], P('sp', 'dp')
- down_grad: float32 [1024, 2048], P('dp', 'sp')
- kernel_grad: float32 [31, 1024], P(None, 'dp')
- bias_grad: float32 [1024], P('dp')
- gain_grad: float32 [1024], P('dp')
- shift_grad: float32 [1024], P('dp')
All inputs are finite; a program needn't handle non-finite values.
Results may differ from a plain program's by a relative error of at most 0.006.
Values may be sent and summed in bfloat16 or wider, within the bound.
A program may use at most 64 MiB of HBM per device.

v0:
```python
import math
import jax
import jax.numpy as jnp
from jax import lax
from jax.sharding import PartitionSpec as P

EPS = 1e-05


def with_halo(block, sides, width):
    for axis, dim in sides:
        count = lax.axis_size(axis)
        forward = [(i, i + 1) for i in range(count - 1)]
        backward = [(target, source) for source, target in forward]
        low = lax.ppermute(
            lax.slice_in_dim(block, block.shape[dim] - width, None, axis=dim), axis, forward
        )
        high = lax.ppermute(lax.slice_in_dim(block, 0, width, axis=dim), axis, backward)
        block = jnp.concatenate([low, block, high], axis=dim)
    return block


def project(weight, rows):
    return lax.dot_general(
        weight, rows, (((0,), (1,)), ((), ())), preferred_element_type=jnp.float32
    )


def on_device(
    normed_input,
    out_grad,
    value_weight,
    gate_weight,
    down_weight,
    conv_kernel,
    conv_bias,
    norm_gain,
    norm_shift,
):
    tokens = normed_input.shape[0]
    width = conv_kernel.shape[0]
    reach = width // 2
    local_channels = value_weight.shape[1]
    channels = local_channels * lax.axis_size("dp")
    ratio = 1.0 / math.sqrt(tokens * lax.axis_size("sp"))
    value_b = project(value_weight, normed_input).astype(jnp.bfloat16)
    gate_b = project(gate_weight, normed_input).astype(jnp.bfloat16)
    value = lax.optimization_barrier(value_b).astype(jnp.float32)
    gate = lax.optimization_barrier(gate_b).astype(jnp.float32)
    opening = jax.nn.sigmoid(gate)
    glu = value * opening
    padded = with_halo(glu, (("sp", 1),), reach)
    mixed = jnp.zeros_like(glu) + conv_bias[:, None]
    for tap in range(width):
        mixed = mixed + conv_kernel[tap][:, None] * padded[:, tap : tap + tokens]
    total, squares = lax.psum((jnp.sum(mixed, axis=0), jnp.sum(mixed * mixed, axis=0)), "dp")
    mean = total / channels
    spread = squares / channels - mean * mean
    inv_std = lax.rsqrt(spread + EPS)
    centred = (mixed - mean[None, :]) * inv_std[None, :]
    normed = centred * norm_gain[:, None] + norm_shift[:, None]
    sig = jax.nn.sigmoid(normed)
    activated = (normed * sig).astype(jnp.bfloat16)
    d_act = lax.dot_general(
        down_weight, out_grad, (((1,), (1,)), ((), ())), preferred_element_type=jnp.float32
    )
    d_normed = d_act * sig * (1.0 + normed * (1.0 - sig))
    d_centred = d_normed * norm_gain[:, None]
    first, second = lax.psum(
        (jnp.sum(d_centred, axis=0), jnp.sum(d_centred * centred, axis=0)), "dp"
    )
    d_mixed = inv_std[None, :] * (
        d_centred - first[None, :] / channels - centred * (second[None, :] / channels)
    )
    d_padded = with_halo(d_mixed, (("sp", 1),), reach)
    d_glu = jnp.zeros_like(d_mixed)
    for tap in range(width):
        d_glu = (
            d_glu
            + conv_kernel[tap][:, None] * d_padded[:, 2 * reach - tap : 2 * reach - tap + tokens]
        )
    kernel_local = jnp.stack(
        [jnp.sum(d_mixed * padded[:, tap : tap + tokens], axis=1) for tap in range(width)]
    )
    kernel_grad, bias_grad, gain_grad, shift_grad = lax.psum(
        (
            kernel_local * ratio,
            jnp.sum(d_mixed, axis=1) * ratio,
            jnp.sum(d_normed * centred, axis=1) * ratio,
            jnp.sum(d_normed, axis=1) * ratio,
        ),
        "sp",
    )
    d_value = (d_glu * opening).astype(jnp.bfloat16)
    d_gate = (d_glu * value * opening * (1.0 - opening)).astype(jnp.bfloat16)
    numbers = (((0,), (1,)), ((), ()))
    value_part = lax.dot_general(normed_input, d_value, numbers, preferred_element_type=jnp.float32)
    gate_part = lax.dot_general(normed_input, d_gate, numbers, preferred_element_type=jnp.float32)
    down_part = lax.dot_general(out_grad, activated, numbers, preferred_element_type=jnp.float32)
    summed = lax.psum_scatter(
        jnp.concatenate([value_part, gate_part, down_part], axis=1) * ratio,
        "sp",
        scatter_dimension=0,
        tiled=True,
    )
    value_grad = summed[:, :local_channels]
    gate_grad = summed[:, local_channels : 2 * local_channels]
    down_grad = summed[:, 2 * local_channels :].T
    numbers = (((0,), (1,)), ((), ()))
    own = lax.dot_general(d_value, value_weight, numbers, preferred_element_type=jnp.float32)
    own = own + lax.dot_general(d_gate, gate_weight, numbers, preferred_element_type=jnp.float32)
    input_grad = lax.psum(own, "dp").astype(jnp.bfloat16)
    return (
        input_grad,
        value_grad,
        gate_grad,
        down_grad,
        kernel_grad,
        bias_grad,
        gain_grad,
        shift_grad,
    )


def solution(mesh):
    in_specs = (
        P("sp", None),
        P("sp", None),
        P(None, "dp"),
        P(None, "dp"),
        P("dp", None),
        P(None, "dp"),
        P("dp"),
        P("dp"),
        P("dp"),
    )
    out_specs = (
        P("sp", None),
        P("sp", "dp"),
        P("sp", "dp"),
        P("dp", "sp"),
        P(None, "dp"),
        P("dp"),
        P("dp"),
        P("dp"),
    )
    return jax.shard_map(
        on_device, mesh=mesh, in_specs=in_specs, out_specs=out_specs, check_vma=False
    )
```

profile of v0, /device:TPU:0, one launch (start us, length us, event | category | flops | bytes accessed | tf_op | source)
XLA Modules:
  0.0 185.2 jit_solution(6150821379646648669)
XLA Ops:
  7.2 1.2 copy-done
  8.5 1.7 convolution_convert_fusion.1
  10.9 4.9 %collective-permute-start = (f32[256,15]{0,1:T(8,128)S(1)}, f32[256,15]{0,1:T(8,128)S(1)}, u32[]{:S(2)}, u32[]{:S(2)}) collective-permute-start(f32[256,15]{0,1:T(8,128)S(1)} %get-tuple-element.71), channel_id=1, source_target_pairs={{0,4},{4,8},{8,12},{12,16},{16,20},{20,24},{24,28},{1,5},{5,9},{9,... | collective-permute-start | bytes 46088 | tf_op jit(solution)/shard_map/ppermute | solution.py:15
  15.8 1.3 collective-permute-start.1
  17.2 4.2 %collective-permute-done.1 = f32[256,15]{0,1:T(8,128)S(1)} collective-permute-done((f32[256,15]{0,1:T(8,128)S(1)}, f32[256,15]{0,1:T(8,128)S(1)}, u32[]{:S(2)}, u32[]{:S(2)}) %collective-permute-start.1) | collective-permute-done | bytes 15392 | tf_op jit(solution)/shard_map/ppermute | solution.py:18
  21.4 1.7 multiply_reduce_fusion.33
  23.2 5.7 %all-reduce.2 = (f32[320]{0:T(512)S(1)}, f32[320]{0:T(512)S(1)}) all-reduce(f32[320]{0:T(512)S(1)} %get-tuple-element.53, f32[320]{0:T(512)S(1)} %get-tuple-element.52), channel_id=1, replica_groups=mesh['sp'=8,'dp'=4] {'dp'}, use_global_device_ids=true, to_apply=%region_3.0 | all-reduce | flops 640 | bytes 5120 | tf_op jit(solution)/shard_map/psum | solution.py:56
  28.8 2.4 %multiply_reduce_fusion = (f32[256]{0:T(256)S(1)}, f32[320]{0:T(512)S(1)}, f32[320]{0:T(512)S(1)}, f32[256]{0:T(256)S(1)}, f32[256,320]{0,1:T(8,128)S(1)}) fusion(f32[256,320]{0,1:T(8,128)S(1)} %get-tuple-element.65, f32[320]{0:T(512)S(1)} %get-tuple-element.105, f32[320]{0:T(512)S(1)} %get-tuple-element.104, f32[256]{0:T(256)S(1)} %copy-done.4, ...), kind=kOutput, calls=%fused_computation.214 | convolution fusion | flops 337099648 | bytes 3023872 | tf_op jit(solution)/shard_map/dot_general | solution.py:64
  31.2 6.6 %all-reduce.1 = (f32[320]{0:T(512)S(1)}, f32[320]{0:T(512)S(1)}) all-reduce(f32[320]{0:T(512)S(1)} %get-tuple-element.47, f32[320]{0:T(512)S(1)} %get-tuple-element.48), channel_id=1, replica_groups=mesh['sp'=8,'dp'=4] {'dp'}, use_global_device_ids=true, to_apply=%region_7.0 | all-reduce | flops 640 | bytes 5120 | tf_op jit(solution)/shard_map/psum | solution.py:69
  38.4 1.3 collective-permute-start.2
  39.7 5.0 %collective-permute-start.3 = (f32[256,15]{0,1:T(8,128)S(1)}, f32[256,15]{0,1:T(8,128)S(1)}, u32[]{:S(2)}, u32[]{:S(2)}) collective-permute-start(f32[256,15]{0,1:T(8,128)S(1)} %get-tuple-element.70), channel_id=1, source_target_pairs={{0,4},{4,8},{8,12},{12,16},{16,20},{20,24},{24,28},{1,5},{5,9},{9,... | collective-permute-start | bytes 46088 | tf_op jit(solution)/shard_map/ppermute | solution.py:15
  44.7 2.2 %convolution_bitcast_fusion = f32[2048,256]{0,1:T(8,128)S(1)} fusion(bf16[320,2048]{1,0:T(8,128)(2,1)} %param.10, f32[256,320]{0,1:T(8,128)S(1)} %get-tuple-element.65, f32[256]{0:T(256)S(1)} %copy-done.6, f32[256]{0:T(256)S(1)} %copy-done.4, f32[320]{0:T(512)S(1)} %get-tuple-element.105, f32[320]{0:T(512)S(1)} %get-tuple-element.104), kind=kOutput, calls=%fused_computation.2 | convolution fusion | flops 336281600 | bytes 3740160 | tf_op jit(solution)/shard_map/dot_general | solution.py:99
  46.9 1.7 fusion.3
  48.6 0.7 convolution_bitcast_fusion.1
  49.3 0.8 convolution_bitcast_fusion.2
  50.1 3.3 %maximum_multiply_fusion = f32[2048,768]{0,1:T(8,128)} fusion(f32[2048,256]{0,1:T(8,128)S(1)} %convolution_bitcast_fusion, f32[2048,256]{0,1:T(8,128)S(1)} %convolution_bitcast_fusion.1, f32[2048,256]{0,1:T(8,128)S(1)} %convolution_bitcast_fusion.2), kind=kLoop, calls=%fused_computation | loop fusion | flops 4718592 | bytes 12582912 | tf_op jit(solution)/shard_map/mul | solution.py:101
  54.6 40.4 %all-reduce = (f32[31,256]{1,0:T(8,128)}, f32[256]{0:T(256)}, f32[256]{0:T(256)}, f32[256]{0:T(256)}) all-reduce(f32[31,256]{1,0:T(8,128)S(1)} %broadcast_multiply_fusion, f32[256]{0:T(256)S(1)} %broadcast_multiply_fusion.6, f32[256]{0:T(256)S(1)} %get-tuple-element.108, ...), channel_id=1, replica_groups=mesh['sp'=8,'dp'=4] {'sp'}, use_global_device_ids=true, to_apply=%region_41.0 | all-reduce | flops 8704 | bytes 69632 | tf_op jit(solution)/shard_map/psum | solution.py:85
  95.0 1.8 fusion.126
  96.8 2.1 %convolution_add_fusion = f32[320,2048]{1,0:T(8,128)} fusion(f32[320,2048]{1,0:T(8,128)S(1)} %fusion.126, bf16[256,320]{0,1:T(8,128)(2,1)S(1)} %get-tuple-element.63, bf16[2048,256]{1,0:T(8,128)(2,1)S(1)} %copy-done.2), kind=kOutput, calls=%fused_computation.1 | convolution fusion | flops 336199680 | bytes 6455296 | tf_op jit(solution)/shard_map/dot_general | solution.py:111
  98.9 50.2 %all-reduce.4 = bf16[320,2048]{1,0:T(8,128)(2,1)} all-reduce(f32[320,2048]{1,0:T(8,128)} %convolution_add_fusion), channel_id=1, replica_groups=mesh['sp'=8,'dp'=4] {'dp'}, use_global_device_ids=true, to_apply=%region_8.0 | all-reduce | flops 655360 | bytes 3932160 | tf_op jit(solution)/shard_map/psum | solution.py:112
  149.1 25.7 %reduce-scatter.2.cloned.1.call-done = f32[256,768]{0,1:T(8,128)} async-done(((f32[2048,768]{0,1:T(8,128)}), f32[256,768]{0,1:T(8,128)}) %reduce-scatter.2.cloned.1.call-update) | async-done | bytes 786448 | tf_op jit(solution)/shard_map/reduce_scatter | solution.py:100
  174.8 1.9 %slice_bitcast_fusion = (f32[256,256]{1,0:T(8,128)}, f32[256,256]{0,1:T(8,128)S(1)}, f32[256,256]{0,1:T(8,128)S(1)}) fusion(f32[256,768]{0,1:T(8,128)} %reduce-scatter.2.cloned.1.call-done), kind=kLoop, calls=%fused_computation.257 | loop fusion | bytes 1572864 | tf_op jit(solution)/shard_map/transpose | solution.py:108
  176.6 0.8 copy.18
  177.5 0.8 copy.17
  (34 shorter events, 2.5 us)
Async XLA Ops:
  7.2 1.3 copy-start
  7.2 3.0 %copy-start.1 = (bf16[2048,256]{1,0:T(8,128)(2,1)S(1)}, bf16[2048,256]{1,0:T(8,128)(2,1)}, u32[]{:S(2)}) copy-start(bf16[2048,256]{1,0:T(8,128)(2,1)} %param.12) | copy-start | bytes 3145732
  7.2 167.6 %reduce-scatter.2.cloned.1.call-start = ((), (), s32[]{:S(2)}) async-start(), calls=%async_computation.1 | async-start | bytes 7077888 | tf_op jit(solution)/shard_map/reduce_scatter | solution.py:100
  10.2 6.9 %copy-start.3 = (f32[31,256]{1,0:T(8,128)S(1)}, f32[31,256]{1,0:T(8,128)}, u32[]{:S(2)}) copy-start(f32[31,256]{1,0:T(8,128)} %param.14) | copy-start | bytes 95236
  10.2 11.2 %copy-start.5 = (f32[256]{0:T(256)S(1)}, f32[256]{0:T(256)}, u32[]{:S(2)}) copy-start(f32[256]{0:T(256)} %param.15) | copy-start | bytes 3076
  10.3 18.6 %copy-start.4 = (f32[256]{0:T(256)S(1)}, f32[256]{0:T(256)}, u32[]{:S(2)}) copy-start(f32[256]{0:T(256)} %param.16) | copy-start | bytes 3076
  10.3 18.6 %copy-start.6 = (f32[256]{0:T(256)S(1)}, f32[256]{0:T(256)}, u32[]{:S(2)}) copy-start(f32[256]{0:T(256)} %param.17) | copy-start | bytes 3076
  10.9 6.3 %collective-permute-start = (f32[256,15]{0,1:T(8,128)S(1)}, f32[256,15]{0,1:T(8,128)S(1)}, u32[]{:S(2)}, u32[]{:S(2)}) collective-permute-start(f32[256,15]{0,1:T(8,128)S(1)} %get-tuple-element.71), channel_id=1, source_target_pairs={{0,4},{4,8},{8,12},{12,16},{16,20},{20,24},{24,28},{1,5},{5,9},{9,... | collective-permute-start | bytes 46088 | tf_op jit(solution)/shard_map/ppermute | solution.py:15
  15.8 5.6 %collective-permute-start.1 = (f32[256,15]{0,1:T(8,128)S(1)}, f32[256,15]{0,1:T(8,128)S(1)}, u32[]{:S(2)}, u32[]{:S(2)}) collective-permute-start(f32[256,15]{0,1:T(8,128)S(1)} %get-tuple-element.72), channel_id=1, source_target_pairs={{4,0},{8,4},{12,8},{16,12},{20,16},{24,20},{28,24},{5,1},{9,5},{13... | collective-permute-start | bytes 46088 | tf_op jit(solution)/shard_map/ppermute | solution.py:18
  38.4 8.5 %collective-permute-start.2 = (f32[256,15]{0,1:T(8,128)S(1)}, f32[256,15]{0,1:T(8,128)S(1)}, u32[]{:S(2)}, u32[]{:S(2)}) collective-permute-start(f32[256,15]{0,1:T(8,128)S(1)} %get-tuple-element.69), channel_id=1, source_target_pairs={{4,0},{8,4},{12,8},{16,12},{20,16},{24,20},{28,24},{5,1},{9,5},{13... | collective-permute-start | bytes 46088 | tf_op jit(solution)/shard_map/ppermute | solution.py:18
  39.7 7.2 %collective-permute-start.3 = (f32[256,15]{0,1:T(8,128)S(1)}, f32[256,15]{0,1:T(8,128)S(1)}, u32[]{:S(2)}, u32[]{:S(2)}) collective-permute-start(f32[256,15]{0,1:T(8,128)S(1)} %get-tuple-element.70), channel_id=1, source_target_pairs={{0,4},{4,8},{8,12},{12,16},{16,20},{20,24},{24,28},{1,5},{5,9},{9,... | collective-permute-start | bytes 46088 | tf_op jit(solution)/shard_map/ppermute | solution.py:15
  54.6 42.2 %copy-start.2 = (bf16[2048,256]{1,0:T(8,128)(2,1)S(1)}, bf16[2048,256]{1,0:T(8,128)(2,1)}, u32[]{:S(2)}) copy-start(bf16[2048,256]{1,0:T(8,128)(2,1)} %param.12) | copy-start | bytes 3145732
Sparse Core Ops, SparseCore 0:
  53.5 121.1 reduce-scatter.1
where the time goes:
time: 186 us; the launch traced here: 185 us
  blocking collectives  103 us (55%)
  waiting for transfers between devices  30 us (16%)
  between operations  14.3 us (8%)
  starting transfers between devices  12.5 us (7%)
  matrix products  12.2 us (7%)
  other arithmetic  8.41 us (5%)
  local copies, waits for them, and re-layouts  4.97 us (3%)
    psum x1, blocking collectives, on_device(): input_grad = lax.psum(own, 'dp').astype(jnp.bfloat16)  50.2 us
    psum x1, blocking collectives, on_device(): lax.psum((kernel_local * ratio, jnp.sum(d_mixed, axis=1) * ratio, jnp.sum...  40.4 us
    reduce_scatter x1, waiting for transfers between devices, on_device(): lax.psum_scatter(jnp.concatenate([value_part, gate_part, down_part], axis...  25.7 us
    ppermute x2, starting transfers between devices, with_halo(): lax.ppermute(lax.slice_in_dim(block, block.shape[dim] - width, None, axis...  9.85 us
    psum x1, blocking collectives, on_device(): lax.psum((jnp.sum(d_centred, axis=0), jnp.sum(d_centred * centred, axis=0...  6.65 us
    psum x1, blocking collectives, on_device(): lax.psum((jnp.sum(mixed, axis=0), jnp.sum(mixed * mixed, axis=0)), 'dp')  5.67 us
    ppermute x2, waiting for transfers between devices, with_halo(): lax.ppermute(lax.slice_in_dim(block, 0, width, axis=dim), axis, backward)  4.21 us
  transfers between devices with their start and end apart: 5, of which 3 were waited for; matrix products, arithmetic and copies ran while one was open for 4% of the time, Pallas kernels for 0%

commit v1 on v0

--- a/solution.py
+++ b/solution.py
@@ -109,7 +109,13 @@
     numbers = (((0,), (1,)), ((), ()))
     own = lax.dot_general(d_value, value_weight, numbers, preferred_element_type=jnp.float32)
     own = own + lax.dot_general(d_gate, gate_weight, numbers, preferred_element_type=jnp.float32)
-    input_grad = lax.psum(own, "dp").astype(jnp.bfloat16)
+
+    def cards_launch(page, a_name="dp"):
+        block_now = lax.all_gather(page, a_name)
+        a_next = jnp.sum(block_now, axis=0)
+        return a_next
+
+    input_grad = cards_launch(own).astype(jnp.bfloat16)
     return (
         input_grad,
         value_grad,

time: 186 us -> 194 us (1.043)
  waiting for transfers between devices: 30 us -> 80 us
  blocking collectives: 103 us -> 53.1 us
  other arithmetic: 8.41 us -> 14.9 us
    psum x1 -> x0, blocking collectives: 50.2 us -> none  [on_device(): input_grad = lax.psum(own, 'dp').astype(jnp.bfloat16)]
    reduce_scatter x1, waiting for transfers between devices: 25.7 us -> 75.7 us  [on_device(): lax.psum_scatter(jnp.concatenate([value_part, gate_part, down_part], axis...]
    reduce_sum x0 -> x1, other arithmetic: none -> 6.54 us  [cards_launch(): a_next = jnp.sum(block_now, axis=0)]
  transfers between devices with their start and end apart: 5 -> 6, of which waited for: 3 -> 3; matrix products, arithmetic and copies ran while one was open for 4% -> 6% of each run, Pallas kernels for 0% -> 0%
where the time goes in v1:
time: 194 us; the launch traced here: 193 us
  waiting for transfers between devices  80 us (41%)
  blocking collectives  53.1 us (27%)
  between operations  15.7 us (8%)
  other arithmetic  14.9 us (8%)
  starting transfers between devices  12.5 us (6%)
  matrix products  12.2 us (6%)
  local copies, waits for them, and re-layouts  4.97 us (3%)
    reduce_scatter x1, waiting for transfers between devices, on_device(): lax.psum_scatter(jnp.concatenate([value_part, gate_part, down_part], axis...  75.7 us
    psum x1, blocking collectives, on_device(): lax.psum((kernel_local * ratio, jnp.sum(d_mixed, axis=1) * ratio, jnp.sum...  40.8 us
    ppermute x2, starting transfers between devices, with_halo(): lax.ppermute(lax.slice_in_dim(block, block.shape[dim] - width, None, axis...  9.86 us
    psum x1, blocking collectives, on_device(): lax.psum((jnp.sum(d_centred, axis=0), jnp.sum(d_centred * centred, axis=0...  6.65 us
    reduce_sum x1, other arithmetic, cards_launch(): a_next = jnp.sum(block_now, axis=0)  6.54 us
    psum x1, blocking collectives, on_device(): lax.psum((jnp.sum(mixed, axis=0), jnp.sum(mixed * mixed, axis=0)), 'dp')  5.67 us
    ppermute x2, waiting for transfers between devices, with_halo(): lax.ppermute(lax.slice_in_dim(block, 0, width, axis=dim), axis, backward)  4.21 us
  transfers between devices with their start and end apart: 6, of which 3 were waited for; matrix products, arithmetic and copies ran while one was open for 6% of the time, Pallas kernels for 0%

profile of v1, /device:TPU:0, one launch (start us, length us, event | category | flops | bytes accessed | tf_op | source)
XLA Modules:
  0.0 193.4 jit_solution(15434672136551521440)
XLA Ops:
  8.1 1.2 copy-done
  9.3 1.7 convolution_convert_fusion.1
  11.7 4.9 %collective-permute-start = (f32[256,15]{0,1:T(8,128)S(1)}, f32[256,15]{0,1:T(8,128)S(1)}, u32[]{:S(2)}, u32[]{:S(2)}) collective-permute-start(f32[256,15]{0,1:T(8,128)S(1)} %get-tuple-element.71), channel_id=1, source_target_pairs={{0,4},{4,8},{8,12},{12,16},{16,20},{20,24},{24,28},{1,5},{5,9},{9,... | collective-permute-start | bytes 46088 | tf_op jit(solution)/shard_map/ppermute | solution.py:15
  16.6 1.3 collective-permute-start.1
  18.1 4.2 %collective-permute-done.1 = f32[256,15]{0,1:T(8,128)S(1)} collective-permute-done((f32[256,15]{0,1:T(8,128)S(1)}, f32[256,15]{0,1:T(8,128)S(1)}, u32[]{:S(2)}, u32[]{:S(2)}) %collective-permute-start.1) | collective-permute-done | bytes 15392 | tf_op jit(solution)/shard_map/ppermute | solution.py:18
  22.3 1.7 multiply_reduce_fusion.33
  24.0 5.7 %all-reduce.2 = (f32[320]{0:T(512)S(1)}, f32[320]{0:T(512)S(1)}) all-reduce(f32[320]{0:T(512)S(1)} %get-tuple-element.53, f32[320]{0:T(512)S(1)} %get-tuple-element.52), channel_id=1, replica_groups=mesh['sp'=8,'dp'=4] {'dp'}, use_global_device_ids=true, to_apply=%region_3.0 | all-reduce | flops 640 | bytes 5120 | tf_op jit(solution)/shard_map/psum | solution.py:56
  29.7 2.4 %multiply_reduce_fusion = (f32[256]{0:T(256)S(1)}, f32[320]{0:T(512)S(1)}, f32[320]{0:T(512)S(1)}, f32[256]{0:T(256)S(1)}, f32[256,320]{0,1:T(8,128)S(1)}) fusion(f32[256,320]{0,1:T(8,128)S(1)} %get-tuple-element.65, f32[320]{0:T(512)S(1)} %get-tuple-element.105, f32[320]{0:T(512)S(1)} %get-tuple-element.104, f32[256]{0:T(256)S(1)} %copy-done.4, ...), kind=kOutput, calls=%fused_computation.214 | convolution fusion | flops 337099648 | bytes 3023872 | tf_op jit(solution)/shard_map/dot_general | solution.py:64
  32.0 6.7 %all-reduce.1 = (f32[320]{0:T(512)S(1)}, f32[320]{0:T(512)S(1)}) all-reduce(f32[320]{0:T(512)S(1)} %get-tuple-element.47, f32[320]{0:T(512)S(1)} %get-tuple-element.48), channel_id=1, replica_groups=mesh['sp'=8,'dp'=4] {'dp'}, use_global_device_ids=true, to_apply=%region_7.0 | all-reduce | flops 640 | bytes 5120 | tf_op jit(solution)/shard_map/psum | solution.py:69
  39.2 1.3 collective-permute-start.2
  40.5 5.0 %collective-permute-start.3 = (f32[256,15]{0,1:T(8,128)S(1)}, f32[256,15]{0,1:T(8,128)S(1)}, u32[]{:S(2)}, u32[]{:S(2)}) collective-permute-start(f32[256,15]{0,1:T(8,128)S(1)} %get-tuple-element.70), channel_id=1, source_target_pairs={{0,4},{4,8},{8,12},{12,16},{16,20},{20,24},{24,28},{1,5},{5,9},{9,... | collective-permute-start | bytes 46088 | tf_op jit(solution)/shard_map/ppermute | solution.py:15
  45.5 2.2 %convolution_bitcast_fusion = f32[2048,256]{0,1:T(8,128)S(1)} fusion(bf16[320,2048]{1,0:T(8,128)(2,1)} %param.10, f32[256,320]{0,1:T(8,128)S(1)} %get-tuple-element.65, f32[256]{0:T(256)S(1)} %copy-done.6, f32[256]{0:T(256)S(1)} %copy-done.4, f32[320]{0:T(512)S(1)} %get-tuple-element.105, f32[320]{0:T(512)S(1)} %get-tuple-element.104), kind=kOutput, calls=%fused_computation.2 | convolution fusion | flops 336281600 | bytes 3740160 | tf_op jit(solution)/shard_map/dot_general | solution.py:99
  47.7 1.7 fusion.3
  49.5 0.7 convolution_bitcast_fusion.1
  50.2 0.8 convolution_bitcast_fusion.2
  50.9 3.3 %maximum_multiply_fusion = f32[2048,768]{0,1:T(8,128)} fusion(f32[2048,256]{0,1:T(8,128)S(1)} %convolution_bitcast_fusion, f32[2048,256]{0,1:T(8,128)S(1)} %convolution_bitcast_fusion.1, f32[2048,256]{0,1:T(8,128)S(1)} %convolution_bitcast_fusion.2), kind=kLoop, calls=%fused_computation | loop fusion | flops 4718592 | bytes 12582912 | tf_op jit(solution)/shard_map/mul | solution.py:101
  54.3 1.9 fusion.126
  56.2 2.1 %convolution_add_fusion = f32[320,2048]{1,0:T(8,128)} fusion(f32[320,2048]{1,0:T(8,128)S(1)} %fusion.126, bf16[256,320]{0,1:T(8,128)(2,1)S(1)} %get-tuple-element.63, bf16[2048,256]{1,0:T(8,128)(2,1)S(1)} %copy-done.2), kind=kOutput, calls=%fused_computation.1 | convolution fusion | flops 336199680 | bytes 6455296 | tf_op jit(solution)/shard_map/dot_general | solution.py:111
  59.4 40.8 %all-reduce = (f32[31,256]{1,0:T(8,128)}, f32[256]{0:T(256)}, f32[256]{0:T(256)}, f32[256]{0:T(256)}) all-reduce(f32[31,256]{1,0:T(8,128)S(1)} %broadcast_multiply_fusion, f32[256]{0:T(256)S(1)} %broadcast_multiply_fusion.6, f32[256]{0:T(256)S(1)} %get-tuple-element.108, ...), channel_id=1, replica_groups=mesh['sp'=8,'dp'=4] {'sp'}, use_global_device_ids=true, to_apply=%region_41.0 | all-reduce | flops 8704 | bytes 69632 | tf_op jit(solution)/shard_map/psum | solution.py:85
  100.2 75.7 %reduce-scatter.2.cloned.1.call-done = f32[256,768]{0,1:T(8,128)} async-done(((f32[2048,768]{0,1:T(8,128)}), f32[256,768]{0,1:T(8,128)}) %reduce-scatter.2.cloned.1.call-update) | async-done | bytes 786448 | tf_op jit(solution)/shard_map/reduce_scatter | solution.py:100
  175.9 1.9 slice_bitcast_fusion
  177.8 0.8 copy.18
  178.6 0.8 copy.17
  179.4 6.5 %reduce_sum.355 = bf16[320,2048]{1,0:T(8,128)(2,1)} reduce(f32[4,320,2048]{2,1,0:T(8,128)} %bitcast.84, f32[]{:T(128)} %constant.6.clone.1), dimensions={0}, to_apply=%region_8.0 | reduce | flops 1966080 | bytes 11796484 | tf_op jit(solution)/shard_map/reduce_sum | solution.py:115
  (37 shorter events, 2.6 us)
Async XLA Ops:
  8.0 1.3 copy-start
  8.0 3.0 %copy-start.1 = (bf16[2048,256]{1,0:T(8,128)(2,1)S(1)}, bf16[2048,256]{1,0:T(8,128)(2,1)}, u32[]{:S(2)}) copy-start(bf16[2048,256]{1,0:T(8,128)(2,1)} %param.12) | copy-start | bytes 3145732
  8.0 167.9 %reduce-scatter.2.cloned.1.call-start = ((), (), s32[]{:S(2)}) async-start(), calls=%async_computation.1 | async-start | bytes 7077888 | tf_op jit(solution)/shard_map/reduce_scatter | solution.py:100
  11.1 6.9 %copy-start.3 = (f32[31,256]{1,0:T(8,128)S(1)}, f32[31,256]{1,0:T(8,128)}, u32[]{:S(2)}) copy-start(f32[31,256]{1,0:T(8,128)} %param.14) | copy-start | bytes 95236
  11.1 11.2 %copy-start.5 = (f32[256]{0:T(256)S(1)}, f32[256]{0:T(256)}, u32[]{:S(2)}) copy-start(f32[256]{0:T(256)} %param.15) | copy-start | bytes 3076
  11.1 18.6 %copy-start.4 = (f32[256]{0:T(256)S(1)}, f32[256]{0:T(256)}, u32[]{:S(2)}) copy-start(f32[256]{0:T(256)} %param.16) | copy-start | bytes 3076
  11.1 18.6 %copy-start.6 = (f32[256]{0:T(256)S(1)}, f32[256]{0:T(256)}, u32[]{:S(2)}) copy-start(f32[256]{0:T(256)} %param.17) | copy-start | bytes 3076
  11.7 6.3 %collective-permute-start = (f32[256,15]{0,1:T(8,128)S(1)}, f32[256,15]{0,1:T(8,128)S(1)}, u32[]{:S(2)}, u32[]{:S(2)}) collective-permute-start(f32[256,15]{0,1:T(8,128)S(1)} %get-tuple-element.71), channel_id=1, source_target_pairs={{0,4},{4,8},{8,12},{12,16},{16,20},{20,24},{24,28},{1,5},{5,9},{9,... | collective-permute-start | bytes 46088 | tf_op jit(solution)/shard_map/ppermute | solution.py:15
  16.6 5.6 %collective-permute-start.1 = (f32[256,15]{0,1:T(8,128)S(1)}, f32[256,15]{0,1:T(8,128)S(1)}, u32[]{:S(2)}, u32[]{:S(2)}) collective-permute-start(f32[256,15]{0,1:T(8,128)S(1)} %get-tuple-element.72), channel_id=1, source_target_pairs={{4,0},{8,4},{12,8},{16,12},{20,16},{24,20},{28,24},{5,1},{9,5},{13... | collective-permute-start | bytes 46088 | tf_op jit(solution)/shard_map/ppermute | solution.py:18
  39.2 8.5 %collective-permute-start.2 = (f32[256,15]{0,1:T(8,128)S(1)}, f32[256,15]{0,1:T(8,128)S(1)}, u32[]{:S(2)}, u32[]{:S(2)}) collective-permute-start(f32[256,15]{0,1:T(8,128)S(1)} %get-tuple-element.69), channel_id=1, source_target_pairs={{4,0},{8,4},{12,8},{16,12},{20,16},{24,20},{28,24},{5,1},{9,5},{13... | collective-permute-start | bytes 46088 | tf_op jit(solution)/shard_map/ppermute | solution.py:18
  40.5 7.2 %collective-permute-start.3 = (f32[256,15]{0,1:T(8,128)S(1)}, f32[256,15]{0,1:T(8,128)S(1)}, u32[]{:S(2)}, u32[]{:S(2)}) collective-permute-start(f32[256,15]{0,1:T(8,128)S(1)} %get-tuple-element.70), channel_id=1, source_target_pairs={{0,4},{4,8},{8,12},{12,16},{16,20},{20,24},{24,28},{1,5},{5,9},{9,... | collective-permute-start | bytes 46088 | tf_op jit(solution)/shard_map/ppermute | solution.py:15
  54.2 125.2 %all-gather.3.cloned.1.call-start = ((), (), s32[]{:S(2)}) async-start(), calls=%async_computation.2 | async-start | bytes 13107200 | tf_op jit(solution)/shard_map/all_gather | solution.py:114
  54.3 1.9 copy-start.2
Sparse Core Ops, SparseCore 0:
  54.3 121.5 reduce-scatter.1
Sparse Core Ops, SparseCore 1:
  58.3 71.9 all-gather.2
